TPU v7x, 128 devices: a whole 4x4x4 slice. The times are simulated.
128 devices in a mesh: rep: 2 (over z_hi), fs: 32 (over z_lo, y, x), tp: 2 (over core).
Axes of the slice: x: 4, y: 4, z: 4 (z_hi: 2, z_lo: 2; z = z_hi * 2 + z_lo), core: 2. Of those that a mesh axis runs over, the one named last changes fastest.
Arguments:
- tokens: bfloat16 [65536, 2048], P(('rep', 'fs')), may hold values from -6 to 6
- norm_mix: bfloat16 [2048], replicated, may hold values from 0.099609375 to 1.8984375
- w_unit: bfloat16 [2048, 1024], P('fs', 'tp'), may hold values from -0.125 to 0.125
- w_value: bfloat16 [2048, 1024], P('fs', 'tp'), may hold values from -0.125 to 0.125
- spatial: bfloat16 [4, 128, 128], replicated, may hold values from -0.52734375 to 0.52734375
- spatial_bias: bfloat16 [4, 128], replicated, may hold values from 0.099609375 to 1.8984375
- group_gain: bfloat16 [1024], replicated, may hold values from 0.099609375 to 1.8984375
- group_shift: bfloat16 [1024], replicated, may hold values from -3 to 3
- w_mix_out: bfloat16 [1024, 2048], P('tp', 'fs'), may hold values from -0.1875 to 0.1875
- norm_ffn: bfloat16 [2048], replicated, may hold values from 0.099609375 to 1.8984375
- w_gate: bfloat16 [2048, 2816], P('fs', 'tp'), may hold values from -0.125 to 0.125
- w_up: bfloat16 [2048, 2816], P('fs', 'tp'), may hold values from -0.125 to 0.125
- w_down: bfloat16 [2816, 2048], P('tp', 'fs'), may hold values from -0.109375 to 0.109375
Outputs:
- layer_out: bfloat16 [65536, 2048], P(('rep', 'fs', 'tp'))
All inputs are finite; a program needn't handle non-finite values.
Results may differ from a plain program's by a relative error of at most 0.008.
Values may be sent and summed in bfloat16 or wider, within the bound.
No kernel may reach another device: no remote copies, remote signals or barrier semaphores. Data moves between devices by JAX's collectives and lax.ppermute only.
A program may use at most 128 MiB of HBM per device.

v0:
```python
import jax
import jax.numpy as jnp
from jax import lax
from jax.sharding import PartitionSpec as P


def sent_together(arrays, axis, dim, along):
    ends, at = ([], 0)
    for a in arrays[:-1]:
        at += a.shape[along]
        ends.append(at)
    both = jnp.concatenate(arrays, axis=along)
    return tuple(jnp.split(lax.all_gather(both, axis, axis=dim, tiled=True), ends, axis=along))


def sent_to_all(x, axis):
    copies = jnp.broadcast_to(x, (lax.axis_size(axis), *x.shape))
    return lax.all_to_all(copies, axis, split_axis=0, concat_axis=0, tiled=True)


def in_order(pieces, dim):
    pieces = jnp.moveaxis(pieces, 0, dim)
    dims = pieces.shape
    return pieces.reshape(*dims[:dim], dims[dim] * dims[dim + 1], *dims[dim + 2 :])


def gathered_copies(x, axis, dim):
    pieces = sent_to_all(x, axis)
    return in_order(pieces, dim)


def total_of_pieces(x, axis):
    return lax.all_gather(x, axis).sum(0)


def split_up(x, dim, peers):
    before, after = (x.shape[:dim], x.shape[dim + 1 :])
    return jnp.moveaxis(x.reshape(*before, peers, -1, *after), dim, 0)


def summed_on_arrival(x, axis, dim):
    pieces = split_up(x, dim, lax.axis_size(axis))
    arrived = lax.all_to_all(pieces, axis, split_axis=0, concat_axis=0, tiled=True)
    return arrived.astype(jnp.float32).sum(axis=0)


def rms_scale(values, gain):
    values = values.astype(jnp.float32)
    scale = lax.rsqrt(jnp.mean(values * values, axis=-1, keepdims=True) + 1e-06)
    return values * scale * gain.astype(jnp.float32)


def spatial_unit(unit_pre, value_pre, spatial, spatial_bias, group_gain, group_shift):
    count, width = value_pre.shape
    groups = spatial.shape[0]
    block = spatial.shape[1]
    active = jax.nn.gelu(value_pre, approximate=True).reshape(count, groups, width // groups)
    center = jnp.mean(active, axis=-1, keepdims=True)
    spread = jnp.mean(jnp.square(active - center), axis=-1, keepdims=True)
    normal = ((active - center) * lax.rsqrt(spread + 1e-06)).reshape(count, width)
    normal = normal * group_gain.astype(jnp.float32) + group_shift.astype(jnp.float32)
    grouped = normal.astype(jnp.bfloat16)
    causal = jnp.tril(jnp.ones((block, block), dtype=bool))
    weights = jnp.where(causal[None], spatial, jnp.zeros_like(spatial))
    tiles = grouped.reshape(count // block, block, groups, width // groups)
    mixed = jnp.einsum("gts,nsgd->ntgd", weights, tiles, preferred_element_type=jnp.float32)
    mixed = mixed + spatial_bias.astype(jnp.float32).T[None, :, :, None]
    return jax.nn.gelu(unit_pre, approximate=True) * mixed.reshape(count, width)


def on_device(
    tokens,
    norm_mix,
    w_unit,
    w_value,
    spatial,
    spatial_bias,
    group_gain,
    group_shift,
    w_mix_out,
    norm_ffn,
    w_gate,
    w_up,
    w_down,
):
    count = tokens.shape[0]
    half = count // lax.axis_size("tp")
    position = lax.axis_index("tp")
    row_start = position * half
    local_width = w_unit.shape[1]
    group_count = spatial.shape[0] // lax.axis_size("tp")
    group_start = position * group_count
    spatial_local = lax.dynamic_slice_in_dim(spatial, group_start, group_count, 0)
    bias_local = lax.dynamic_slice_in_dim(spatial_bias, group_start, group_count, 0)
    gain_local = lax.dynamic_slice_in_dim(group_gain, position * local_width, local_width, 0)
    shift_local = lax.dynamic_slice_in_dim(group_shift, position * local_width, local_width, 0)
    normed = rms_scale(tokens, norm_mix).astype(jnp.bfloat16)
    unit_whole, value_whole = sent_together((w_unit, w_value), "fs", 0, 1)
    unit_pre = jnp.dot(normed, unit_whole, preferred_element_type=jnp.float32)
    value_pre = jnp.dot(normed, value_whole, preferred_element_type=jnp.float32)
    gated = spatial_unit(
        unit_pre, value_pre, spatial_local, bias_local, gain_local, shift_local
    ).astype(jnp.bfloat16)
    partial_terms = jnp.dot(
        gated, gathered_copies(w_mix_out, "fs", 1), preferred_element_type=jnp.float32
    )
    summed = total_of_pieces(partial_terms, "tp")
    h_mid = (tokens.astype(jnp.float32) + summed).astype(jnp.bfloat16)
    normed_mid = rms_scale(h_mid, norm_ffn).astype(jnp.bfloat16)
    gate_whole, up_whole = sent_together((w_gate, w_up), "fs", 0, 1)
    gate = jnp.dot(normed_mid, gate_whole, preferred_element_type=jnp.float32)
    up = jnp.dot(normed_mid, up_whole, preferred_element_type=jnp.float32)
    hidden = (jax.nn.silu(gate) * up).astype(jnp.bfloat16)
    down_cols = lax.all_gather(w_down, "fs", axis=1, tiled=True)
    residual_rows = lax.dynamic_slice_in_dim(h_mid, row_start, half, 0).astype(jnp.float32)
    summed_rows = summed_on_arrival(
        jnp.dot(hidden, down_cols, preferred_element_type=jnp.float32).astype(jnp.bfloat16), "tp", 0
    )
    return (residual_rows + summed_rows).astype(jnp.bfloat16)


def solution(mesh):
    placed = (
        P(("rep", "fs"), None),
        P(),
        P("fs", "tp"),
        P("fs", "tp"),
        P(),
        P(),
        P(),
        P(),
        P("tp", "fs"),
        P(),
        P("fs", "tp"),
        P("fs", "tp"),
        P("tp", "fs"),
    )
    return jax.shard_map(
        on_device,
        mesh=mesh,
        in_specs=placed,
        out_specs=P(("rep", "fs", "tp"), None),
        check_vma=False,
    )
```

profile of v0, /device:TPU:1, one launch (start us, length us, event | category | flops | bytes accessed | tf_op | source)
XLA Modules:
  0.0 629.2 jit_solution(16438548954573870074)
XLA Ops:
  6.5 0.0 copy-start.5
  6.5 0.0 copy-start.9
  6.5 0.0 copy-start.8
  6.5 0.0 copy-start.7
  6.5 0.0 all-gather.6.cloned.1.call-start
  6.6 1.6 pad_maximum_fusion.1
  8.1 0.0 all-gather.6.cloned.1.call-update
  8.2 2.4 broadcast_in_dim.13
  10.6 9.3 %all-to-all-start = ((bf16[32,512,64]{1,2,0:T(8,128)(2,1)}), bf16[32,512,64]{1,2,0:T(8,128)(2,1)}, u32[]{:S(2)}, u32[]{:S(2)}) async-start(bf16[32,512,64]{1,2,0:T(8,128)(2,1)} %broadcast_in_dim.13), calls=%async_computation | async-start | bytes 4194304 | tf_op jit(solution)/shard_map/all_to_all | solution.py:18
  19.9 0.0 all-gather.12.cloned.1.call-start
  20.0 0.0 copy-done.5
  20.0 0.0 copy-done.9
  20.0 0.0 copy-done.8
  20.0 0.0 copy-done.7
  20.0 0.1 dynamic-slice_convert_fusion
  20.1 3.1 fusion.3
  23.3 133.9 %all-gather.6.cloned.1.call-done = bf16[2048,1024]{1,0:T(8,128)(2,1)} async-done(((bf16[64,1024]{1,0:T(8,128)(2,1)}), bf16[2048,1024]{1,0:T(8,128)(2,1)}) %all-gather.6.cloned.1.call-update) | async-done | bytes 4194320 | tf_op jit(solution)/shard_map/all_gather | solution.py:13
  157.1 6.9 %fusion.35 = f32[1024,512]{1,0:T(8,128)} fusion(bf16[2048,1024]{1,0:T(8,128)(2,1)} %all-gather.6.cloned.1.call-done, bf16[1024,2048]{1,0:T(8,128)(2,1)} %param.13, f32[2048]{0:T(1024)S(1)} %convert_element_type.51, f32[1024]{0:T(1024)S(1)} %add_rsqrt_fusion.2), kind=kOutput, calls=%fused_computation.39 | convolution fusion | flops 2160066560 | bytes 8400896 | tf_op jit(solution)/shard_map/dot_general | solution.py:100
  164.1 2.6 reshape.58
  166.7 1.2 reduce_sum.55
  167.9 14.4 %multiply_reduce_fusion = f32[1024,2]{1,0:T(8,128)S(1)} fusion(f32[1024,2,256]{2,1,0:T(2,128)S(1)} %reshape.58, f32[1024,2]{1,0:T(8,128)S(1)} %broadcast_multiply_fusion), kind=kLoop, calls=%fused_computation.46 | loop fusion | flops 1570816 | bytes 2113536 | tf_op jit(solution)/shard_map/reduce_sum | solution.py:59
  182.3 0.1 add_rsqrt_fusion
  182.4 1.2 mul.112
  183.6 0.2 copy.32
  183.8 0.0 copy-start.1
  183.8 1.2 sub.17
  185.1 0.2 copy.31
  185.3 0.2 copy-done.1
  185.4 0.0 copy-start.4
  185.4 0.8 add_convert_fusion.1
  186.2 0.3 reshape.59
  186.5 0.0 copy-done.4
  186.5 0.5 bitcast_add_fusion
  187.1 2.4 copy.28
  189.5 1.8 copy.33
  191.2 0.0 all-to-all-done
  191.3 11.6 %fusion.51 = f32[1024,2048]{1,0:T(8,128)} fusion(bf16[512,2048]{0,1:T(8,128)(2,1)} %bitcast.5, f32[1024,512]{1,0:T(8,128)S(1)} %bitcast.30, bf16[2048,1024]{1,0:T(8,128)(2,1)} %all-gather.6.cloned.1.call-done, bf16[1024,2048]{1,0:T(8,128)(2,1)} %param.13, f32[2048]{0:T(1024)S(1)} %convert_element_type.51, f32[1024]{0:T(1024)S(1)} %add_rsqrt_fusion.2), kind=kOutput, calls=%fused_computation.47 | convolution fusion | flops 4308598784 | bytes 18886656 | tf_op jit(solution)/shard_map/dot_general | solution.py:104
  202.9 0.0 copy-start.2
  202.9 0.0 copy-start.3
  202.9 0.0 copy-start.6
  202.9 0.0 all-gather.12.cloned.1.call-update
  202.9 0.0 all-gather.8.cloned.1.call-start
  203.0 0.8 copy-done.2
  203.8 0.1 copy-done.3
  203.9 0.8 pad_maximum_fusion
  204.6 0.0 all-gather.8.cloned.1.call-update
  204.7 0.0 all-gather.10.cloned.1.call-start
  204.7 0.5 all-gather.10.cloned.1.call-update
  205.2 0.0 copy-done.6
  205.3 49.1 %all-gather.12.cloned.1.call-done = f32[2048,2048]{1,0:T(8,128)} async-done(((f32[1024,2048]{1,0:T(8,128)}), f32[2048,2048]{1,0:T(8,128)}) %all-gather.12.cloned.1.call-update) | async-done | bytes 16777232 | tf_op jit(solution)/shard_map/all_gather | solution.py:33
  254.4 11.8 %reduce_sum.57 = f32[1024,2048]{1,0:T(8,128)} reduce(f32[2,1024,2048]{2,1,0:T(8,128)} %bitcast.23, f32[]{:T(128)} %constant.15.clone.1), dimensions={0}, to_apply=%region_3.4 | reduce | flops 2097152 | bytes 25165828 | tf_op jit(solution)/shard_map/reduce_sum | solution.py:33
  266.1 7.8 %fusion = (f32[1024]{0:T(1024)S(1)}, bf16[1024,2048]{1,0:T(8,128)(2,1)}) fusion(f32[1024,2048]{1,0:T(8,128)} %reduce_sum.57, bf16[1024,2048]{1,0:T(8,128)(2,1)} %param.13), kind=kLoop, calls=%fused_computation.5 | loop fusion | flops 12581888 | bytes 16781312 | tf_op jit(solution)/shard_map/reduce_sum | solution.py:49
  273.9 135.7 %all-gather.8.cloned.1.call-done = bf16[2048,2816]{1,0:T(8,128)(2,1)} async-done(((bf16[64,2816]{1,0:T(8,128)(2,1)}), bf16[2048,2816]{1,0:T(8,128)(2,1)}) %all-gather.8.cloned.1.call-update) | async-done | bytes 11534352 | tf_op jit(solution)/shard_map/all_gather | solution.py:13
  409.6 11.9 %fusion.9 = f32[1024,1408]{1,0:T(8,128)} fusion(bf16[2048,2816]{1,0:T(8,128)(2,1)} %all-gather.8.cloned.1.call-done, bf16[1024,2048]{1,0:T(8,128)(2,1)} %get-tuple-element.6, f32[2048]{0:T(1024)S(1)} %convert_element_type.60, f32[1024]{0:T(1024)S(1)} %add_rsqrt_fusion.1), kind=kOutput, calls=%fused_computation.15 | convolution fusion | flops 5913968640 | bytes 15740928 | tf_op jit(solution)/shard_map/dot_general | solution.py:111
  421.5 147.9 %all-gather.10.cloned.1.call-done = bf16[1408,2048]{0,1:T(8,128)(2,1)} async-done(((bf16[1408,64]{0,1:T(8,128)(2,1)}), bf16[1408,2048]{0,1:T(8,128)(2,1)}) %all-gather.10.cloned.1.call-update) | async-done | bytes 5767184 | tf_op jit(solution)/shard_map/all_gather | solution.py:114
  569.4 20.9 %fusion.16 = bf16[1024,2048]{1,0:T(8,128)(2,1)} fusion(bf16[1408,2048]{0,1:T(8,128)(2,1)} %all-gather.10.cloned.1.call-done, f32[1024,1408]{1,0:T(8,128)} %fusion.9, bf16[2048,2816]{1,0:T(8,128)(2,1)} %all-gather.8.cloned.1.call-done, bf16[1024,2048]{1,0:T(8,128)(2,1)} %get-tuple-element.6, f32[2048]{0:T(1024)S(1)} %convert_element_type.60, ...), kind=kOutput, calls=%fused_computation.20 | convolution fusion | flops 11830296576 | bytes 25702400 | tf_op jit(solution)/shard_map/dot_general | solution.py:117
  590.3 28.2 %all_to_all.10 = bf16[2,512,2048]{2,1,0:T(8,128)(2,1)S(1)} all-to-all(bf16[2,512,2048]{2,1,0:T(8,128)(2,1)} %bitcast.29), channel_id=1, replica_groups=mesh['rep'=2,'fs'=32,'tp'=2] {'tp'}, dimensions={0} | all-to-all | bytes 8388608 | tf_op jit(solution)/shard_map/all_to_all | solution.py:43
  618.5 0.0 copy-start
  618.5 1.0 convert_reduce_fusion
  619.4 1.2 copy-done
  620.7 2.1 add_convert_fusion
  (7 shorter events, 0.1 us)
Async XLA Ops:
  6.5 13.4 %copy-start.5 = (bf16[2048]{0:T(1024)(128)(2,1)S(1)}, bf16[2048]{0:T(1024)(128)(2,1)}, u32[]{:S(2)}) copy-start(bf16[2048]{0:T(1024)(128)(2,1)} %param.14) | copy-start | bytes 12292
  6.5 13.5 %copy-start.9 = (bf16[4,128]{1,0:T(4,128)(2,1)S(1)}, bf16[4,128]{1,0:T(4,128)(2,1)}, u32[]{:S(2)}) copy-start(bf16[4,128]{1,0:T(4,128)(2,1)} %param.18) | copy-start | bytes 3076
  6.5 13.5 %copy-start.8 = (bf16[1024]{0:T(1024)(128)(2,1)S(1)}, bf16[1024]{0:T(1024)(128)(2,1)}, u32[]{:S(2)}) copy-start(bf16[1024]{0:T(1024)(128)(2,1)} %param.19) | copy-start | bytes 6148
  6.5 13.5 %copy-start.7 = (bf16[1024]{0:T(1024)(128)(2,1)S(1)}, bf16[1024]{0:T(1024)(128)(2,1)}, u32[]{:S(2)}) copy-start(bf16[1024]{0:T(1024)(128)(2,1)} %param.20) | copy-start | bytes 6148
  6.5 150.6 %all-gather.6.cloned.1.call-start = ((), (), s32[]{:S(2)}) async-start(), calls=%async_computation.2 | async-start | bytes 4325376 | tf_op jit(solution)/shard_map/all_gather | solution.py:13
  10.6 180.7 %all-to-all-start = ((bf16[32,512,64]{1,2,0:T(8,128)(2,1)}), bf16[32,512,64]{1,2,0:T(8,128)(2,1)}, u32[]{:S(2)}, u32[]{:S(2)}) async-start(bf16[32,512,64]{1,2,0:T(8,128)(2,1)} %broadcast_in_dim.13), calls=%async_computation | async-start | bytes 4194304 | tf_op jit(solution)/shard_map/all_to_all | solution.py:18
  19.9 234.4 %all-gather.12.cloned.1.call-start = ((), (), s32[]{:S(2)}) async-start(), calls=%async_computation.5 | async-start | bytes 25165824 | tf_op jit(solution)/shard_map/all_gather | solution.py:33
  183.8 1.6 copy-start.1
  185.4 1.1 copy-start.4
  202.9 0.9 copy-start.2
  202.9 1.0 copy-start.3
  202.9 2.4 copy-start.6
  202.9 206.7 %all-gather.8.cloned.1.call-start = ((), (), s32[]{:S(2)}) async-start(), calls=%async_computation.3 | async-start | bytes 11894784 | tf_op jit(solution)/shard_map/all_gather | solution.py:13
  204.7 364.7 %all-gather.10.cloned.1.call-start = ((), (), s32[]{:S(2)}) async-start(), calls=%async_computation.4 | async-start | bytes 5947392 | tf_op jit(solution)/shard_map/all_gather | solution.py:114
  618.5 2.2 copy-start
Sparse Core Ops, SparseCore 0:
  9.0 148.1 all-gather.5
  203.0 51.2 all-gather.11
  256.0 153.5 all-gather.7
  411.1 158.2 all-gather.9
where the time goes:
time: 630 us; the launch traced here: 629 us
  waiting for transfers between devices  467 us (74%)
  matrix products  51.8 us (8%)
  other arithmetic  44.6 us (7%)
  blocking collectives  28.2 us (4%)
  local copies, waits for them, and re-layouts  14.5 us (2%)
  between operations  13.3 us (2%)
  starting transfers between devices  9.5 us (2%)
    all_gather x2, waiting for transfers between devices, sent_together(): lax.all_gather(both, axis, axis=dim, tiled=True)  270 us
    all_gather x1, waiting for transfers between devices, on_device(): down_cols = lax.all_gather(w_down, 'fs', axis=1, tiled=True)  148 us
    all_gather x1, waiting for transfers between devices, total_of_pieces(): return lax.all_gather(x, axis).sum(0)  49.1 us
    all_to_all x1, blocking collectives, summed_on_arrival(): lax.all_to_all(pieces, axis, split_axis=0, concat_axis=0, tiled=True)  28.2 us
    dot_general x1, matrix products, on_device(): jnp.dot(hidden, down_cols, preferred_element_type=jnp.float32)  20.9 us
    reduce_sum x1, other arithmetic, spatial_unit(): spread = jnp.mean(jnp.square(active - center), axis=-1, keepdims=True)  14.4 us
  transfers between devices with their start and end apart: 5, of which 4 were waited for; matrix products, arithmetic and copies ran while one was open for 11% of the time, Pallas kernels for 0%

commit v1 on v0

--- a/solution.py
+++ b/solution.py
@@ -111,7 +111,8 @@
     gate = jnp.dot(normed_mid, gate_whole, preferred_element_type=jnp.float32)
     up = jnp.dot(normed_mid, up_whole, preferred_element_type=jnp.float32)
     hidden = (jax.nn.silu(gate) * up).astype(jnp.bfloat16)
-    down_cols = lax.all_gather(w_down, "fs", axis=1, tiled=True)
+    parts = lax.all_gather(w_down, "fs")
+    down_cols = jnp.concatenate(parts, axis=1)
     residual_rows = lax.dynamic_slice_in_dim(h_mid, row_start, half, 0).astype(jnp.float32)
     summed_rows = summed_on_arrival(
         jnp.dot(hidden, down_cols, preferred_element_type=jnp.float32).astype(jnp.bfloat16), "tp", 0

time: 630 us -> 600 us (0.952)
  waiting for transfers between devices: 467 us -> 429 us
  local copies, waits for them, and re-layouts: 14.5 us -> 22.5 us
    all_gather x1, waiting for transfers between devices: 148 us -> 113 us  [on_device(): parts = lax.all_gather(w_down, 'fs')]
  transfers between devices with their start and end apart: 5 -> 5, of which waited for: 4 -> 4; matrix products, arithmetic and copies ran while one was open for 11% -> 13% of each run, Pallas kernels for 0% -> 0%
where the time goes in v1:
time: 600 us
  waiting for transfers between devices  429 us (72%)
  matrix products  51.9 us (9%)
  other arithmetic  44.6 us (7%)
  blocking collectives  28.2 us (5%)
  local copies, waits for them, and re-layouts  22.5 us (4%)
  between operations  13.4 us (2%)
  starting transfers between devices  9.5 us (2%)
    all_gather x2, waiting for transfers between devices, sent_together(): lax.all_gather(both, axis, axis=dim, tiled=True)  269 us
    all_gather x1, waiting for transfers between devices, on_device(): parts = lax.all_gather(w_down, 'fs')  113 us
    all_gather x1, waiting for transfers between devices, total_of_pieces(): return lax.all_gather(x, axis).sum(0)  47 us
    all_to_all x1, blocking collectives, summed_on_arrival(): lax.all_to_all(pieces, axis, split_axis=0, concat_axis=0, tiled=True)  28.2 us
    dot_general x1, matrix products, on_device(): jnp.dot(hidden, down_cols, preferred_element_type=jnp.float32)  20.9 us
    reduce_sum x1, other arithmetic, spatial_unit(): spread = jnp.mean(jnp.square(active - center), axis=-1, keepdims=True)  14.4 us
  transfers between devices with their start and end apart: 5, of which 4 were waited for; matrix products, arithmetic and copies ran while one was open for 13% of the time, Pallas kernels for 0%

profile of v1, /device:TPU:1, one launch (start us, length us, event | category | flops | bytes accessed | tf_op | source)
XLA Modules:
  0.0 599.6 jit_solution(1685834223399084839)
XLA Ops:
  6.5 0.0 copy-start.5
  6.5 0.0 copy-start.9
  6.5 0.0 copy-start.8
  6.5 0.0 copy-start.7
  6.5 0.0 all-gather.7.cloned.1.call-start
  6.6 1.6 pad_maximum_fusion.1
  8.1 0.0 all-gather.7.cloned.1.call-update
  8.2 0.0 all-gather.13.cloned.1.call-start
  8.2 0.7 all-gather.13.cloned.1.call-update
  8.9 2.4 broadcast_in_dim.13
  11.3 9.3 %all-to-all-start = ((bf16[32,512,64]{1,2,0:T(8,128)(2,1)}), bf16[32,512,64]{1,2,0:T(8,128)(2,1)}, u32[]{:S(2)}, u32[]{:S(2)}) async-start(bf16[32,512,64]{1,2,0:T(8,128)(2,1)} %broadcast_in_dim.13), calls=%async_computation | async-start | bytes 4194304 | tf_op jit(solution)/shard_map/all_to_all | solution.py:18
  20.7 0.0 all-gather.11.cloned.1.call-start
  20.7 0.0 copy-done.5
  20.7 0.0 copy-done.9
  20.8 0.0 copy-done.8
  20.8 0.0 copy-done.7
  20.8 0.1 dynamic-slice_convert_fusion
  20.9 3.1 fusion.3
  24.0 133.0 %all-gather.7.cloned.1.call-done = bf16[2048,1024]{1,0:T(8,128)(2,1)} async-done(((bf16[64,1024]{1,0:T(8,128)(2,1)}), bf16[2048,1024]{1,0:T(8,128)(2,1)}) %all-gather.7.cloned.1.call-update) | async-done | bytes 4194320 | tf_op jit(solution)/shard_map/all_gather | solution.py:13
  157.0 6.9 %fusion.35 = f32[1024,512]{1,0:T(8,128)} fusion(bf16[2048,1024]{1,0:T(8,128)(2,1)} %all-gather.7.cloned.1.call-done, bf16[1024,2048]{1,0:T(8,128)(2,1)} %param.13, f32[2048]{0:T(1024)S(1)} %convert_element_type.51, f32[1024]{0:T(1024)S(1)} %add_rsqrt_fusion.2), kind=kOutput, calls=%fused_computation.39 | convolution fusion | flops 2160066560 | bytes 8400896 | tf_op jit(solution)/shard_map/dot_general | solution.py:100
  163.9 2.6 reshape.64
  166.5 1.2 reduce_sum.55
  167.7 14.4 %multiply_reduce_fusion = f32[1024,2]{1,0:T(8,128)S(1)} fusion(f32[1024,2,256]{2,1,0:T(2,128)S(1)} %reshape.64, f32[1024,2]{1,0:T(8,128)S(1)} %broadcast_multiply_fusion), kind=kLoop, calls=%fused_computation.46 | loop fusion | flops 1570816 | bytes 2113536 | tf_op jit(solution)/shard_map/reduce_sum | solution.py:59
  182.2 0.1 add_rsqrt_fusion
  182.3 1.2 mul.112
  183.5 0.2 copy.40
  183.7 0.0 copy-start.1
  183.7 1.2 sub.17
  184.9 0.2 copy.39
  185.1 0.2 copy-done.1
  185.3 0.0 copy-start.4
  185.3 0.8 add_convert_fusion.1
  186.1 0.3 reshape.65
  186.4 0.0 copy-done.4
  186.4 0.5 bitcast_add_fusion
  186.9 2.4 copy.35
  189.3 1.8 copy.41
  191.1 0.0 all-to-all-done
  191.1 11.7 %fusion.51 = f32[1024,2048]{1,0:T(8,128)} fusion(bf16[512,2048]{0,1:T(8,128)(2,1)} %bitcast.5, f32[1024,512]{1,0:T(8,128)S(1)} %bitcast.40, bf16[2048,1024]{1,0:T(8,128)(2,1)} %all-gather.7.cloned.1.call-done, bf16[1024,2048]{1,0:T(8,128)(2,1)} %param.13, f32[2048]{0:T(1024)S(1)} %convert_element_type.51, f32[1024]{0:T(1024)S(1)} %add_rsqrt_fusion.2), kind=kOutput, calls=%fused_computation.47 | convolution fusion | flops 4308598784 | bytes 18886656 | tf_op jit(solution)/shard_map/dot_general | solution.py:104
  202.8 0.0 copy-start.2
  202.8 0.0 copy-start.3
  202.8 0.0 copy-start.6
  202.8 0.0 all-gather.11.cloned.1.call-update
  202.8 0.0 all-gather.9.cloned.1.call-start
  202.8 0.8 copy-done.2
  203.7 0.1 copy-done.3
  203.8 0.8 pad_maximum_fusion
  204.5 0.0 all-gather.9.cloned.1.call-update
  204.6 0.0 copy-done.6
  204.6 113.1 %all-gather.13.cloned.1.call-done = bf16[45056,64]{0,1:T(8,128)(2,1)} async-done(((bf16[1408,64]{0,1:T(8,128)(2,1)}), bf16[45056,64]{0,1:T(8,128)(2,1)}) %all-gather.13.cloned.1.call-update) | async-done | bytes 5767184 | tf_op jit(solution)/shard_map/all_gather | solution.py:114
  317.7 3.5 copy.42
  321.3 4.5 copy.36
  325.7 47.0 %all-gather.11.cloned.1.call-done = f32[2048,2048]{1,0:T(8,128)} async-done(((f32[1024,2048]{1,0:T(8,128)}), f32[2048,2048]{1,0:T(8,128)}) %all-gather.11.cloned.1.call-update) | async-done | bytes 16777232 | tf_op jit(solution)/shard_map/all_gather | solution.py:33
  372.8 11.8 %reduce_sum.57 = f32[1024,2048]{1,0:T(8,128)} reduce(f32[2,1024,2048]{2,1,0:T(8,128)} %bitcast.31, f32[]{:T(128)} %constant.15.clone.1), dimensions={0}, to_apply=%region_3.4 | reduce | flops 2097152 | bytes 25165828 | tf_op jit(solution)/shard_map/reduce_sum | solution.py:33
  384.5 7.8 %fusion = (f32[1024]{0:T(1024)S(1)}, bf16[1024,2048]{1,0:T(8,128)(2,1)}) fusion(f32[1024,2048]{1,0:T(8,128)} %reduce_sum.57, bf16[1024,2048]{1,0:T(8,128)(2,1)} %param.13), kind=kLoop, calls=%fused_computation.5 | loop fusion | flops 12581888 | bytes 16781312 | tf_op jit(solution)/shard_map/reduce_sum | solution.py:49
  392.3 135.6 %all-gather.9.cloned.1.call-done = bf16[2048,2816]{1,0:T(8,128)(2,1)} async-done(((bf16[64,2816]{1,0:T(8,128)(2,1)}), bf16[2048,2816]{1,0:T(8,128)(2,1)}) %all-gather.9.cloned.1.call-update) | async-done | bytes 11534352 | tf_op jit(solution)/shard_map/all_gather | solution.py:13
  527.8 11.9 %fusion.9 = f32[1024,1408]{1,0:T(8,128)} fusion(bf16[2048,2816]{1,0:T(8,128)(2,1)} %all-gather.9.cloned.1.call-done, bf16[1024,2048]{1,0:T(8,128)(2,1)} %get-tuple-element.6, f32[2048]{0:T(1024)S(1)} %convert_element_type.60, f32[1024]{0:T(1024)S(1)} %add_rsqrt_fusion.1), kind=kOutput, calls=%fused_computation.15 | convolution fusion | flops 5913968640 | bytes 15740928 | tf_op jit(solution)/shard_map/dot_general | solution.py:111
  539.7 20.9 %fusion.16 = bf16[1024,2048]{1,0:T(8,128)(2,1)} fusion(bf16[1408,2048]{0,1:T(8,128)(2,1)} %bitcast.38, f32[1024,1408]{1,0:T(8,128)} %fusion.9, bf16[2048,2816]{1,0:T(8,128)(2,1)} %all-gather.9.cloned.1.call-done, bf16[1024,2048]{1,0:T(8,128)(2,1)} %get-tuple-element.6, f32[2048]{0:T(1024)S(1)} %convert_element_type.60, f32[1024]{0:T(1024)S(1)} %add_rsqrt_fusion.1), kind=kOutput, calls=%fused_computation.20 | convolution fusion | flops 11830296576 | bytes 25702400 | tf_op jit(solution)/shard_map/dot_general | solution.py:118
  560.6 28.2 %all_to_all.10 = bf16[2,512,2048]{2,1,0:T(8,128)(2,1)S(1)} all-to-all(bf16[2,512,2048]{2,1,0:T(8,128)(2,1)} %bitcast.39), channel_id=1, replica_groups=mesh['rep'=2,'fs'=32,'tp'=2] {'tp'}, dimensions={0} | all-to-all | bytes 8388608 | tf_op jit(solution)/shard_map/all_to_all | solution.py:43
  588.8 0.0 copy-start
  588.8 1.0 convert_reduce_fusion
  589.8 1.2 copy-done
  591.0 2.1 add_convert_fusion
  (7 shorter events, 0.1 us)
Async XLA Ops:
  6.5 14.2 %copy-start.5 = (bf16[2048]{0:T(1024)(128)(2,1)S(1)}, bf16[2048]{0:T(1024)(128)(2,1)}, u32[]{:S(2)}) copy-start(bf16[2048]{0:T(1024)(128)(2,1)} %param.14) | copy-start | bytes 12292
  6.5 14.2 %copy-start.9 = (bf16[4,128]{1,0:T(4,128)(2,1)S(1)}, bf16[4,128]{1,0:T(4,128)(2,1)}, u32[]{:S(2)}) copy-start(bf16[4,128]{1,0:T(4,128)(2,1)} %param.18) | copy-start | bytes 3076
  6.5 14.2 %copy-start.8 = (bf16[1024]{0:T(1024)(128)(2,1)S(1)}, bf16[1024]{0:T(1024)(128)(2,1)}, u32[]{:S(2)}) copy-start(bf16[1024]{0:T(1024)(128)(2,1)} %param.19) | copy-start | bytes 6148
  6.5 14.2 %copy-start.7 = (bf16[1024]{0:T(1024)(128)(2,1)S(1)}, bf16[1024]{0:T(1024)(128)(2,1)}, u32[]{:S(2)}) copy-start(bf16[1024]{0:T(1024)(128)(2,1)} %param.20) | copy-start | bytes 6148
  6.5 150.5 %all-gather.7.cloned.1.call-start = ((), (), s32[]{:S(2)}) async-start(), calls=%async_computation.2 | async-start | bytes 4325376 | tf_op jit(solution)/shard_map/all_gather | solution.py:13
  8.2 309.6 %all-gather.13.cloned.1.call-start = ((), (), s32[]{:S(2)}) async-start(), calls=%async_computation.5 | async-start | bytes 5947392 | tf_op jit(solution)/shard_map/all_gather | solution.py:114
  11.3 179.8 %all-to-all-start = ((bf16[32,512,64]{1,2,0:T(8,128)(2,1)}), bf16[32,512,64]{1,2,0:T(8,128)(2,1)}, u32[]{:S(2)}, u32[]{:S(2)}) async-start(bf16[32,512,64]{1,2,0:T(8,128)(2,1)} %broadcast_in_dim.13), calls=%async_computation | async-start | bytes 4194304 | tf_op jit(solution)/shard_map/all_to_all | solution.py:18
  20.7 352.1 %all-gather.11.cloned.1.call-start = ((), (), s32[]{:S(2)}) async-start(), calls=%async_computation.4 | async-start | bytes 25165824 | tf_op jit(solution)/shard_map/all_gather | solution.py:33
  183.7 1.6 copy-start.1
  185.3 1.1 copy-start.4
  202.8 0.9 copy-start.2
  202.8 1.0 copy-start.3
  202.8 1.8 copy-start.6
  202.8 325.0 %all-gather.9.cloned.1.call-start = ((), (), s32[]{:S(2)}) async-start(), calls=%async_computation.3 | async-start | bytes 11894784 | tf_op jit(solution)/shard_map/all_gather | solution.py:13
  588.8 2.2 copy-start
Sparse Core Ops, SparseCore 0:
  9.0 147.9 all-gather.6
  158.7 159.0 all-gather.12
  319.4 53.3 all-gather.10
  374.2 153.5 all-gather.8
